TPU v7x, 32 devices: a whole 2x2x4 slice. The times are simulated.
32 devices in a mesh: dp: 4 (over y, x), kv: 4 (over z), tp: 2 (over core).
Axes of the slice: x: 2, y: 2, z: 4, core: 2. Of those that a mesh axis runs over, the one named last changes fastest.
Arguments:
- tokens: bfloat16 [4, 1024, 1024], P('dp', 'kv', 'tp'), may hold values from -6 to 6
- norm_gain: float32 [1024], replicated, may hold values from 0.1 to 1.9
- w_query: bfloat16 [1024, 1024], P(None, 'tp'), may hold values from -0.1875 to 0.1875
- w_key: bfloat16 [1024, 256], P(None, 'tp'), may hold values from -0.1875 to 0.1875
- w_value: bfloat16 [1024, 256], P(None, 'tp'), may hold values from -0.1875 to 0.1875
- q_gain: float32 [64], replicated, may hold values from 0.1 to 1.9
- k_gain: float32 [64], replicated, may hold values from 0.1 to 1.9
- w_out: bfloat16 [1024, 1024], P('tp'), may hold values from -4 to 4
- chosen: int32 [4, 32, 16], P('dp', 'kv'), may hold values from -1 to 31, as said below
Outputs:
- mixed: bfloat16 [4, 1024, 1024], P('dp', 'kv', 'tp')
- log_total: float32 [4, 16, 1024], P('dp', 'tp', 'kv')
Inputs may be any that keep to these rules, and one draw needn't show every extreme that they name: Each row of chosen (one query block b) holds distinct key block numbers, all at most b, and -1 for empty entries; b itself is always present; a row is full (16 blocks) whenever at least 16 blocks may be chosen by it. Over the 8 rows of one index of kv, the chosen blocks that lie on any one other index of kv are at most 4 distinct ones, and exactly 4 of those on the index just before, for every index but the first. Some blocks are chosen far more often than others.
All inputs are finite; a program needn't handle non-finite values.
Results may differ from a plain program's by a relative error of at most 0.015.
Values may be sent and summed in bfloat16 or wider, within the bound.
A program may use at most 64 MiB of HBM per device.

v0:
```python
import math
import jax
import jax.numpy as jnp
from jax import lax
from jax.sharding import PartitionSpec as P

H = 16
HD = 64
BLK = 32
epsilon = 1e-06
alibi_reach = 4.0
masked = -1e30


def rms_norm(values, gain):
    return (
        values
        * lax.rsqrt(jnp.mean(values * values, axis=-1, keepdims=True) + epsilon)
        * gain.astype(jnp.float32)
    )


def shards(tokens, norm_gain, w_query, w_key, w_value, q_gain, k_gain, w_out, chosen):
    gathered = lax.all_gather(tokens, "tp", axis=2, tiled=True)
    seq_dev, tok_dev, model_width = gathered.shape
    n_kv = lax.axis_size("kv")
    n_tp = lax.axis_size("tp")
    kv_index = lax.axis_index("kv")
    tp_index = lax.axis_index("tp")
    heads_here = w_query.shape[1] // HD
    kv_here = w_key.shape[1] // HD
    group_size = heads_here // kv_here
    blocks_here = tok_dev // BLK
    seq_len = tok_dev * n_kv
    hidden = (
        rms_norm(gathered.astype(jnp.float32), norm_gain)
        .astype(jnp.bfloat16)
        .reshape(seq_dev * tok_dev, model_width)
    )
    queries = rms_norm(
        jnp.dot(hidden, w_query, preferred_element_type=jnp.float32).reshape(
            seq_dev, tok_dev, heads_here, HD
        ),
        q_gain,
    ).astype(jnp.bfloat16)
    key_rows = rms_norm(
        jnp.dot(hidden, w_key, preferred_element_type=jnp.float32).reshape(
            seq_dev, tok_dev, kv_here, HD
        ),
        k_gain,
    ).astype(jnp.bfloat16)
    value_rows = (
        jnp.dot(hidden, w_value, preferred_element_type=jnp.float32)
        .astype(jnp.bfloat16)
        .reshape(seq_dev, tok_dev, kv_here, HD)
    )
    queries = queries.reshape(seq_dev, blocks_here, BLK, kv_here, group_size, HD)
    head_ids = tp_index * heads_here + jnp.arange(heads_here, dtype=jnp.int32)
    slopes = jnp.exp2(-8.0 * (head_ids + 1).astype(jnp.float32) / H).reshape(kv_here, group_size)
    query_pos = (kv_index * tok_dev + jnp.arange(tok_dev, dtype=jnp.int32)).reshape(
        blocks_here, BLK
    )
    score_scale = HD ** (-0.5)

    def absorb(state_now, span_keys, span_values, key_pos, usable):
        row_max, row_sum, weighted = state_now
        key_block = key_pos // BLK
        member = jnp.any(chosen[:, :, :, None] == key_block[:, None, None, :], axis=2)
        offset = query_pos[None, :, :, None] - key_pos[:, None, None, :]
        allowed = member[:, :, None, :] & usable[:, None, None, :] & (offset >= 0)
        scores = (
            jnp.einsum(
                "sbqkgd,snkd->skgbqn", queries, span_keys, preferred_element_type=jnp.float32
            )
            * score_scale
        )
        penalty = (
            slopes[None, :, :, None, None, None]
            * offset.astype(jnp.float32)[:, None, None]
            * alibi_reach
            / seq_len
        )
        scores = jnp.where(allowed[:, None, None], scores - penalty, masked)
        new_max = jnp.maximum(row_max, jnp.max(scores, axis=-1))
        weights = jnp.where(allowed[:, None, None], jnp.exp(scores - new_max[..., None]), 0.0)
        shrink = jnp.exp(row_max - new_max)
        row_sum = row_sum * shrink + jnp.sum(weights, axis=-1)
        weighted = weighted * shrink[..., None] + jnp.einsum(
            "skgbqn,snkd->skgbqd",
            weights.astype(jnp.bfloat16),
            span_values,
            preferred_element_type=jnp.float32,
        )
        return (new_max, row_sum, weighted)

    stat_shape = (seq_dev, kv_here, group_size, blocks_here, BLK)
    initial = (
        jnp.full(stat_shape, masked, jnp.float32),
        jnp.zeros(stat_shape, jnp.float32),
        jnp.zeros(stat_shape + (HD,), jnp.float32),
    )

    def fold_piece(state_now, shard_piece, first_row):
        piece_keys, piece_values = shard_piece
        row_count = piece_keys.shape[1]
        span_len = math.gcd(row_count, tok_dev)

        def one_span(step_index, running):
            first_key = step_index * span_len
            span_keys = lax.dynamic_slice_in_dim(piece_keys, first_key, span_len, 1)
            span_values = lax.dynamic_slice_in_dim(piece_values, first_key, span_len, 1)
            key_pos = jnp.broadcast_to(
                first_row.astype(jnp.int32) + first_key + jnp.arange(span_len, dtype=jnp.int32),
                (seq_dev, span_len),
            )
            return absorb(
                running, span_keys, span_values, key_pos, jnp.ones((seq_dev, span_len), bool)
            )

        return lax.fori_loop(0, row_count // span_len, one_span, state_now)

    row_max, row_sum, weighted = fold_piece(
        initial,
        (
            lax.all_gather(key_rows, "kv", axis=1, tiled=True),
            lax.all_gather(value_rows, "kv", axis=1, tiled=True),
        ),
        jnp.int32(0),
    )
    attended = (weighted / row_sum[..., None]).transpose(0, 3, 4, 1, 2, 5)
    attended = attended.reshape(seq_dev * tok_dev, heads_here * HD).astype(jnp.bfloat16)
    log_total = (row_max + jnp.log(row_sum)).reshape(seq_dev, heads_here, tok_dev)
    own_rows = model_width // n_tp

    def project():
        out_cols = lax.slice_in_dim(w_out, 0, own_rows * lax.axis_size("tp"), axis=1)
        return jnp.dot(attended, out_cols, preferred_element_type=jnp.float32).T

    scattered = lax.psum_scatter(
        project().astype(jnp.bfloat16), "tp", scatter_dimension=0, tiled=True
    ).astype(jnp.float32)
    mixed = scattered.T.reshape(seq_dev, tok_dev, own_rows).astype(jnp.bfloat16)
    return (mixed, log_total)


def solution(mesh):
    in_specs = (
        P("dp", "kv", "tp"),
        P(),
        P(None, "tp"),
        P(None, "tp"),
        P(None, "tp"),
        P(),
        P(),
        P("tp", None),
        P("dp", "kv", None),
    )
    out_specs = (P("dp", "kv", "tp"), P("dp", "tp", "kv"))
    return jax.shard_map(shards, mesh=mesh, in_specs=in_specs, out_specs=out_specs, check_vma=False)
```

profile of v0, /device:TPU:0, one launch (start us, length us, event | category | flops | bytes accessed | tf_op | source)
XLA Modules:
  0.0 81.3 jit_solution(10249953948225324526)
XLA Ops:
  7.2 0.0 copy-start
  7.2 0.0 copy-start.3
  7.2 0.0 copy-start.6
  7.2 0.0 copy-start.4
  7.2 0.0 reduce-scatter.2.cloned.1.call-start
  7.3 2.6 %all_gather.9 = bf16[1,256,1024]{2,1,0:T(8,128)(2,1)S(1)} all-gather(bf16[1,256,512]{2,1,0:T(8,128)(2,1)} %param.11), channel_id=1, replica_groups=mesh['dp'=4,'kv'=4,'tp'=2] {'tp'}, dimensions={2}, use_global_device_ids=true | all-gather | bytes 786432 | tf_op jit(solution)/shard_map/all_gather | solution.py:24
  9.9 0.2 fusion.20
  10.1 1.4 %convolution_convert_fusion.1 = bf16[256,128]{0,1:T(8,128)(2,1)S(1)} fusion(bf16[1024,128]{1,0:T(8,128)(2,1)} %param.15, bf16[1,256,1024]{2,1,0:T(8,128)(2,1)S(1)} %all_gather.9, f32[1024]{0:T(1024)} %param.12, f32[256]{0:T(256)S(1)} %add_rsqrt_fusion.2), kind=kOutput, calls=%fused_computation.39 | convolution fusion | flops 68190208 | bytes 857088 | tf_op jit(solution)/shard_map/dot_general | solution.py:53
  11.5 0.4 fusion.30
  12.0 0.1 multiply_convert_fusion
  12.0 16.2 %all_gather.10 = bf16[1,1024,2,64]{1,3,2,0:T(8,128)(2,1)} all-gather(bf16[1,256,2,64]{1,3,2,0:T(8,128)(2,1)S(1)} %multiply_convert_fusion), channel_id=1, replica_groups=mesh['dp'=4,'kv'=4,'tp'=2] {'kv'}, dimensions={1}, use_global_device_ids=true | all-gather | bytes 327680 | tf_op jit(solution)/shard_map/all_gather | solution.py:125
  28.2 14.6 %all_gather.11 = bf16[1,1024,2,64]{1,3,2,0:T(8,128)(2,1)S(1)} all-gather(bf16[1,256,2,64]{1,3,2,0:T(8,128)(2,1)S(1)} %bitcast.99), channel_id=1, replica_groups=mesh['dp'=4,'kv'=4,'tp'=2] {'kv'}, dimensions={1}, use_global_device_ids=true | all-gather | bytes 327680 | tf_op jit(solution)/shard_map/all_gather | solution.py:126
  42.8 1.3 %fusion.33 = (f32[256,512]{1,0:T(8,128)S(1)}, f32[256,512]{1,0:T(8,128)}) fusion(bf16[1024,512]{1,0:T(8,128)(2,1)S(1)} %copy-done, bf16[1,256,1024]{2,1,0:T(8,128)(2,1)S(1)} %all_gather.9, f32[1024]{0:T(1024)S(1)} %copy-done.3, f32[256]{0:T(256)S(1)} %add_rsqrt_fusion.2), kind=kOutput, calls=%fused_computation.59 | convolution fusion | flops 269615104 | bytes 2626560 | tf_op jit(solution)/shard_map/dot_general | solution.py:41
  44.1 0.2 copy.26
  44.3 0.0 copy-start.2
  44.4 0.1 rsqrt.30
  44.5 1.6 %reshape.336 = f32[1,8,32,2,4,64]{5,4,3,2,1,0:T(4,128)S(1)} reshape(f32[256,512]{1,0:T(8,128)} %get-tuple-element.319) | data formatting | bytes 1048576 | tf_op jit(solution)/shard_map/reshape | solution.py:41
  46.1 1.1 %fusion.24 = bf16[1,8,32,2,4,64]{5,2,4,1,3,0:T(8,128)(2,1)} fusion(f32[1,8,32,2,4,64]{5,4,3,2,1,0:T(4,128)S(1)} %reshape.336, f32[64]{0:T(128)S(1)} %copy-done.5, f32[8,32,2,4]{1,3,0,2:T(4,128)S(1)} %copy.27), kind=kLoop, calls=%fused_computation.45 | loop fusion | flops 393216 | bytes 794880 | tf_op jit(solution)/shard_map/convert_element_type | solution.py:45
  47.2 15.7 %while.20 = (s32[]{:T(128)}, f32[1,2,4,8,32]{4,2,3,1,0:T(4,128)S(1)}, f32[1,2,4,8,32]{4,2,3,1,0:T(4,128)S(1)}, f32[1,2,4,8,32,64]{5,4,3,2,1,0:T(8,128)S(1)}, s32...) while((s32[]{:T(128)}, ...), condition=%wide.region_7.8_spmd.clone, body=%wide.region_3.7_spmd.clone.sunk | while | flops 140261664 | bytes 9419611 | solution.py:120
  47.2 0.1 mul.331
  47.3 0.1 compare_reduce_fusion.2
  47.4 0.1 sub.166
  47.5 0.1 fusion.48
  47.7 0.1 subtract_convert_fusion.2
  47.8 1.7 %fusion.49 = (f32[2,4,8,32]{3,1,2,0:T(4,128)S(1)}, f32[1,2,4,8,32,256]{5,4,2,3,1,0:T(8,128)S(1)}) fusion(f32[8,32,256]{2,1,0:T(8,128)S(1)} %subtract_convert_fusion.2, f32[2,4]{1,0:T(2,128)S(1)} %mul.331, bf16[1,8,32,2,4,64]{5,2,4,1,3,0:T(8,128)(2,1)} %get-tuple-element.431, bf16[1,1024,2,64]{1,3,2,0:T(8,128)(2,1)} %get-tuple-element.430, ...), kind=kOutput, calls=%fused_computation.58.clone.1 | convolution fusion | flops 70252544 | bytes 3022884 | tf_op jit(solution)/shard_map/while/body/eval_jaxpr/sbqkgd,snkd->skgbqn/dot_general | solution.py:72
  49.6 0.8 %fusion.51 = (bf16[2,4,8,32,256]{4,3,1,2,0:T(8,128)(2,1)S(1)}, f32[2,4,8,32]{3,1,2,0:T(4,128)S(1)}) fusion(f32[1,2,4,8,32,256]{5,4,2,3,1,0:T(8,128)S(1)} %get-tuple-element.393, f32[2,4,8,32]{3,1,2,0:T(4,128)S(1)} %bitcast.92, pred[8,32,256]{2,1,0:T(8,128)(4,1)S(1)} %fusion.48), kind=kLoop, calls=%fused_computation.9.clone.1 | loop fusion | flops 2095104 | bytes 3227648 | tf_op jit(solution)/shard_map/reshape.263
  50.4 0.1 bitcast_add_fusion.2
  50.4 0.7 fusion.52
  51.2 0.1 mul.331
  51.3 0.1 compare_reduce_fusion.2
  51.4 0.1 sub.166
  51.5 0.1 fusion.48
  51.6 0.1 subtract_convert_fusion.2
  51.7 1.7 %fusion.49 = (f32[2,4,8,32]{3,1,2,0:T(4,128)S(1)}, f32[1,2,4,8,32,256]{5,4,2,3,1,0:T(8,128)S(1)}) fusion(f32[8,32,256]{2,1,0:T(8,128)S(1)} %subtract_convert_fusion.2, f32[2,4]{1,0:T(2,128)S(1)} %mul.331, bf16[1,8,32,2,4,64]{5,2,4,1,3,0:T(8,128)(2,1)} %get-tuple-element.431, bf16[1,1024,2,64]{1,3,2,0:T(8,128)(2,1)} %get-tuple-element.430, ...), kind=kOutput, calls=%fused_computation.58.clone.1 | convolution fusion | flops 70252544 | bytes 3022884 | tf_op jit(solution)/shard_map/while/body/eval_jaxpr/sbqkgd,snkd->skgbqn/dot_general | solution.py:72
  53.5 0.8 %fusion.51 = (bf16[2,4,8,32,256]{4,3,1,2,0:T(8,128)(2,1)S(1)}, f32[2,4,8,32]{3,1,2,0:T(4,128)S(1)}) fusion(f32[1,2,4,8,32,256]{5,4,2,3,1,0:T(8,128)S(1)} %get-tuple-element.393, f32[2,4,8,32]{3,1,2,0:T(4,128)S(1)} %bitcast.92, pred[8,32,256]{2,1,0:T(8,128)(4,1)S(1)} %fusion.48), kind=kLoop, calls=%fused_computation.9.clone.1 | loop fusion | flops 2095104 | bytes 3227648 | tf_op jit(solution)/shard_map/reshape.263
  54.3 0.1 bitcast_add_fusion.2
  54.4 0.6 fusion.52
  55.1 0.1 mul.331
  55.2 0.1 compare_reduce_fusion.2
  55.3 0.1 sub.166
  55.4 0.1 fusion.48
  55.5 0.1 subtract_convert_fusion.2
  55.6 1.7 %fusion.49 = (f32[2,4,8,32]{3,1,2,0:T(4,128)S(1)}, f32[1,2,4,8,32,256]{5,4,2,3,1,0:T(8,128)S(1)}) fusion(f32[8,32,256]{2,1,0:T(8,128)S(1)} %subtract_convert_fusion.2, f32[2,4]{1,0:T(2,128)S(1)} %mul.331, bf16[1,8,32,2,4,64]{5,2,4,1,3,0:T(8,128)(2,1)} %get-tuple-element.431, bf16[1,1024,2,64]{1,3,2,0:T(8,128)(2,1)} %get-tuple-element.430, ...), kind=kOutput, calls=%fused_computation.58.clone.1 | convolution fusion | flops 70252544 | bytes 3022884 | tf_op jit(solution)/shard_map/while/body/eval_jaxpr/sbqkgd,snkd->skgbqn/dot_general | solution.py:72
  57.4 0.8 %fusion.51 = (bf16[2,4,8,32,256]{4,3,1,2,0:T(8,128)(2,1)S(1)}, f32[2,4,8,32]{3,1,2,0:T(4,128)S(1)}) fusion(f32[1,2,4,8,32,256]{5,4,2,3,1,0:T(8,128)S(1)} %get-tuple-element.393, f32[2,4,8,32]{3,1,2,0:T(4,128)S(1)} %bitcast.92, pred[8,32,256]{2,1,0:T(8,128)(4,1)S(1)} %fusion.48), kind=kLoop, calls=%fused_computation.9.clone.1 | loop fusion | flops 2095104 | bytes 3227648 | tf_op jit(solution)/shard_map/reshape.263
  58.3 0.1 bitcast_add_fusion.2
  58.3 0.6 fusion.52
  59.0 0.1 mul.331
  59.1 0.1 compare_reduce_fusion.2
  59.2 0.1 sub.166
  59.3 0.1 fusion.48
  59.4 0.1 subtract_convert_fusion.2
  59.5 1.7 %fusion.49 = (f32[2,4,8,32]{3,1,2,0:T(4,128)S(1)}, f32[1,2,4,8,32,256]{5,4,2,3,1,0:T(8,128)S(1)}) fusion(f32[8,32,256]{2,1,0:T(8,128)S(1)} %subtract_convert_fusion.2, f32[2,4]{1,0:T(2,128)S(1)} %mul.331, bf16[1,8,32,2,4,64]{5,2,4,1,3,0:T(8,128)(2,1)} %get-tuple-element.431, bf16[1,1024,2,64]{1,3,2,0:T(8,128)(2,1)} %get-tuple-element.430, ...), kind=kOutput, calls=%fused_computation.58.clone.1 | convolution fusion | flops 70252544 | bytes 3022884 | tf_op jit(solution)/shard_map/while/body/eval_jaxpr/sbqkgd,snkd->skgbqn/dot_general | solution.py:72
  61.3 0.8 %fusion.51 = (bf16[2,4,8,32,256]{4,3,1,2,0:T(8,128)(2,1)S(1)}, f32[2,4,8,32]{3,1,2,0:T(4,128)S(1)}) fusion(f32[1,2,4,8,32,256]{5,4,2,3,1,0:T(8,128)S(1)} %get-tuple-element.393, f32[2,4,8,32]{3,1,2,0:T(4,128)S(1)} %bitcast.92, pred[8,32,256]{2,1,0:T(8,128)(4,1)S(1)} %fusion.48), kind=kLoop, calls=%fused_computation.9.clone.1 | loop fusion | flops 2095104 | bytes 3227648 | tf_op jit(solution)/shard_map/reshape.263
  62.2 0.1 bitcast_add_fusion.2
  62.2 0.7 fusion.52
  62.9 0.0 copy-start.1
  62.9 0.3 fusion.26
  63.3 0.4 copy.30
  63.7 0.3 convert_element_type.92
  64.0 0.1 copy-done.1
  64.1 1.2 %fusion.19 = bf16[1024,256]{0,1:T(8,128)(2,1)} fusion(bf16[256,512]{1,0:T(8,128)(2,1)S(1)} %convert_element_type.92, bf16[512,1024]{1,0:T(8,128)(2,1)S(1)} %copy-done.1), kind=kOutput, calls=%fused_computation.38 | convolution fusion | flops 268697600 | bytes 1835008 | tf_op jit(solution)/shard_map/dot_general | solution.py:137
  65.4 0.0 reduce-scatter.2.cloned.1.call-update
  65.4 0.7 reshape.338
  66.1 8.4 %reduce-scatter.2.cloned.1.call-done = bf16[512,256]{0,1:T(8,128)(2,1)} async-done(((bf16[1024,256]{0,1:T(8,128)(2,1)}), bf16[512,256]{0,1:T(8,128)(2,1)}) %reduce-scatter.2.cloned.1.call-update) | async-done | bytes 262160 | tf_op jit(solution)/shard_map/reduce_scatter | solution.py:139
  (43 shorter events, 0.4 us)
Async XLA Ops:
  7.2 35.7 %copy-start = (bf16[1024,512]{1,0:T(8,128)(2,1)S(1)}, bf16[1024,512]{1,0:T(8,128)(2,1)}, u32[]{:S(2)}) copy-start(bf16[1024,512]{1,0:T(8,128)(2,1)} %param.13) | copy-start | bytes 3145732
  7.2 4.3 %copy-start.3 = (f32[1024]{0:T(1024)S(1)}, f32[1024]{0:T(1024)}, u32[]{:S(2)}) copy-start(f32[1024]{0:T(1024)} %param.12) | copy-start | bytes 12292
  7.2 4.3 %copy-start.6 = (bf16[1024,128]{1,0:T(8,128)(2,1)S(1)}, bf16[1024,128]{1,0:T(8,128)(2,1)}, u32[]{:S(2)}) copy-start(bf16[1024,128]{1,0:T(8,128)(2,1)} %param.14) | copy-start | bytes 786436
  7.2 4.7 %copy-start.4 = (f32[64]{0:T(128)S(1)}, f32[64]{0:T(128)}, u32[]{:S(2)}) copy-start(f32[64]{0:T(128)} %param.17) | copy-start | bytes 772
  7.2 67.2 %reduce-scatter.2.cloned.1.call-start = ((), (), s32[]{:S(2)}) async-start(), calls=%async_computation.1 | async-start | bytes 786432 | tf_op jit(solution)/shard_map/reduce_scatter | solution.py:139
  44.1 2.0 %copy-start.5 = (f32[64]{0:T(128)S(1)}, f32[64]{0:T(128)}, u32[]{:S(2)}) copy-start(f32[64]{0:T(128)} %param.16) | copy-start | bytes 772
  44.3 2.9 %copy-start.2 = (s32[1,8,16]{2,1,0:T(8,128)S(1)}, s32[1,8,16]{2,1,0:T(8,128)}, u32[]{:S(2)}) copy-start(s32[1,8,16]{2,1,0:T(8,128)} %param.19) | copy-start | bytes 1540
  62.9 1.2 %copy-start.1 = (bf16[512,1024]{1,0:T(8,128)(2,1)S(1)}, bf16[512,1024]{1,0:T(8,128)(2,1)}, u32[]{:S(2)}) copy-start(bf16[512,1024]{1,0:T(8,128)(2,1)} %param.18) | copy-start | bytes 3145732
Sparse Core Ops, SparseCore 0:
  65.5 8.8 reduce-scatter.1
where the time goes:
time: 81.6 us; the launch traced here: 81.3 us
  blocking collectives  33.4 us (41%)
  between operations  14.3 us (18%)
  matrix products  13.8 us (17%)
  waiting for transfers between devices  8.37 us (10%)
  other arithmetic  6.92 us (8%)
  local copies, waits for them, and re-layouts  4.09 us (5%)
    all_gather x1, blocking collectives, shards(): lax.all_gather(key_rows, 'kv', axis=1, tiled=True)  16.2 us
    all_gather x1, blocking collectives, shards(): lax.all_gather(value_rows, 'kv', axis=1, tiled=True)  14.6 us
    reduce_scatter x1, waiting for transfers between devices, shards(): lax.psum_scatter(project().astype(jnp.bfloat16), 'tp', scatter_dimension=...  8.35 us
    dot_general x4, matrix products, absorb(): jnp.einsum('sbqkgd,snkd->skgbqn', queries, span_keys, preferred_element_t...  6.99 us
    another operation x4, other arithmetic  3.33 us
    all_gather x1, blocking collectives, shards(): gathered = lax.all_gather(tokens, 'tp', axis=2, tiled=True)  2.64 us
    dot_general x4, matrix products, absorb(): jnp.einsum('skgbqn,snkd->skgbqd', weights.astype(jnp.bfloat16), span_valu...  2.6 us
  transfers between devices with their start and end apart: 1, of which 1 were waited for; matrix products, arithmetic and copies ran while one was open for 1% of the time, Pallas kernels for 0%

commit v1 on v0

--- a/solution.py
+++ b/solution.py
@@ -122,7 +122,9 @@
     row_max, row_sum, weighted = fold_piece(
         initial,
         (
-            lax.all_gather(key_rows, "kv", axis=1, tiled=True),
+            jnp.concatenate(
+                lax.all_to_all(jnp.stack([key_rows] * lax.axis_size("kv")), "kv", 0, 0), axis=1
+            ),
             lax.all_gather(value_rows, "kv", axis=1, tiled=True),
         ),
         jnp.int32(0),

time: 81.6 us -> 74.6 us (0.914)
  blocking collectives: 33.4 us -> 17.4 us
  starting transfers between devices: 0.04 us -> 6.23 us
  local copies, waits for them, and re-layouts: 4.09 us -> 5.78 us
    all_gather x1 -> x0, blocking collectives: 16.2 us -> none  [shards(): lax.all_gather(key_rows, 'kv', axis=1, tiled=True)]
    all_to_all x0 -> x1, starting transfers between devices: none -> 6.23 us  [shards(): lax.all_to_all(jnp.stack([key_rows] * lax.axis_size('kv')), 'kv', 0, 0)]
    dot_general x1, matrix products: 0.39 us -> 1.37 us  [shards(): jnp.dot(hidden, w_key, preferred_element_type=jnp.float32)]
    reshape x0 -> x1, local copies, waits for them, and re-layouts: none -> 0.97 us  [shards(): jnp.concatenate(lax.all_to_all(jnp.stack([key_rows] * lax.axis_size('kv')...]
  transfers between devices with their start and end apart: 1 -> 2, of which waited for: 1 -> 1; matrix products, arithmetic and copies ran while one was open for 1% -> 8% of each run, Pallas kernels for 0% -> 0%
where the time goes in v1:
time: 74.6 us; the launch traced here: 74 us
  blocking collectives  17.4 us (23%)
  matrix products  14.4 us (19%)
  between operations  14.2 us (19%)
  waiting for transfers between devices  8.76 us (12%)
  other arithmetic  6.89 us (9%)
  starting transfers between devices  6.23 us (8%)
  local copies, waits for them, and re-layouts  5.78 us (8%)
    all_gather x1, blocking collectives, shards(): lax.all_gather(value_rows, 'kv', axis=1, tiled=True)  14.8 us
    reduce_scatter x1, waiting for transfers between devices, shards(): lax.psum_scatter(project().astype(jnp.bfloat16), 'tp', scatter_dimension=...  8.74 us
    dot_general x4, matrix products, absorb(): jnp.einsum('sbqkgd,snkd->skgbqn', queries, span_keys, preferred_element_t...  6.88 us
    all_to_all x1, starting transfers between devices, shards(): lax.all_to_all(jnp.stack([key_rows] * lax.axis_size('kv')), 'kv', 0, 0)  6.23 us
    another operation x4, other arithmetic  3.31 us
    all_gather x1, blocking collectives, shards(): gathered = lax.all_gather(tokens, 'tp', axis=2, tiled=True)  2.64 us
    dot_general x4, matrix products, absorb(): jnp.einsum('skgbqn,snkd->skgbqd', weights.astype(jnp.bfloat16), span_valu...  2.57 us
    reshape x1, local copies, waits for them, and re-layouts, shards(): jnp.dot(hidden, w_query, preferred_element_type=jnp.float32)  1.59 us
  transfers between devices with their start and end apart: 2, of which 1 were waited for; matrix products, arithmetic and copies ran while one was open for 8% of the time, Pallas kernels for 0%

profile of v1, /device:TPU:0, one launch (start us, length us, event | category | flops | bytes accessed | tf_op | source)
XLA Modules:
  0.0 74.0 jit_solution(16567696017399093974)
XLA Ops:
  7.2 0.0 copy-start
  7.2 0.0 copy-start.3
  7.2 2.6 %all_gather.6 = bf16[1,256,1024]{2,1,0:T(8,128)(2,1)S(1)} all-gather(bf16[1,256,512]{2,1,0:T(8,128)(2,1)} %param.11), channel_id=1, replica_groups=mesh['dp'=4,'kv'=4,'tp'=2] {'tp'}, dimensions={2}, use_global_device_ids=true | all-gather | bytes 786432 | tf_op jit(solution)/shard_map/all_gather | solution.py:24
  9.9 0.2 fusion.20
  10.0 1.4 %bitcast_reduce_fusion.1 = (f32[256,2]{0,1:T(2,128)S(1)}, f32[256,128]{0,1:T(8,128)S(1)}) fusion(bf16[1024,128]{1,0:T(8,128)(2,1)} %param.14, bf16[1,256,1024]{2,1,0:T(8,128)(2,1)S(1)} %all_gather.6, f32[1024]{0:T(1024)} %param.12, f32[256]{0:T(256)S(1)} %add_rsqrt_fusion.2), kind=kOutput, calls=%fused_computation.50 | convolution fusion | flops 68222464 | bytes 924672 | tf_op jit(solution)/shard_map/dot_general | solution.py:47
  11.4 0.1 multiply_convert_fusion
  11.5 0.7 stack.2
  12.3 6.2 %all-to-all-start = ((bf16[4,1,256,2,64]{2,4,3,1,0:T(8,128)(2,1)}), bf16[4,1,256,2,64]{2,4,3,1,0:T(8,128)(2,1)}, u32[]{:S(2)}, u32[]{:S(2)}) async-start(bf16[4,1,256,2,64]{2,4,3,1,0:T(8,128)(2,1)} %stack.2), calls=%async_computation | async-start | bytes 524288 | tf_op jit(solution)/shard_map/all_to_all | solution.py:126
  18.5 1.0 %convolution_convert_fusion.1 = bf16[256,128]{0,1:T(8,128)(2,1)} fusion(bf16[1024,128]{1,0:T(8,128)(2,1)S(1)} %copy-done.6, bf16[1,256,1024]{2,1,0:T(8,128)(2,1)S(1)} %all_gather.6, f32[1024]{0:T(1024)S(1)} %copy-done.3, f32[256]{0:T(256)S(1)} %add_rsqrt_fusion.2), kind=kOutput, calls=%fused_computation.39 | convolution fusion | flops 68190208 | bytes 857088 | tf_op jit(solution)/shard_map/dot_general | solution.py:53
  19.5 1.3 %fusion.33 = (f32[256,512]{1,0:T(8,128)S(1)}, f32[256,512]{1,0:T(8,128)}) fusion(bf16[1024,512]{1,0:T(8,128)(2,1)S(1)} %copy-done, bf16[1,256,1024]{2,1,0:T(8,128)(2,1)S(1)} %all_gather.6, f32[1024]{0:T(1024)S(1)} %copy-done.3, f32[256]{0:T(256)S(1)} %add_rsqrt_fusion.2), kind=kOutput, calls=%fused_computation.59 | convolution fusion | flops 269615104 | bytes 2626560 | tf_op jit(solution)/shard_map/dot_general | solution.py:41
  20.8 0.2 copy.44
  21.0 0.0 copy-start.2
  21.1 0.1 rsqrt.30
  21.2 1.6 %reshape.337 = f32[1,8,32,2,4,64]{5,4,3,2,1,0:T(4,128)S(1)} reshape(f32[256,512]{1,0:T(8,128)} %get-tuple-element.321) | data formatting | bytes 1048576 | tf_op jit(solution)/shard_map/reshape | solution.py:41
  22.8 14.8 %all_gather.7 = bf16[1,1024,2,64]{1,3,2,0:T(8,128)(2,1)S(1)} all-gather(bf16[1,256,2,64]{1,3,2,0:T(8,128)(2,1)} %bitcast.105), channel_id=1, replica_groups=mesh['dp'=4,'kv'=4,'tp'=2] {'kv'}, dimensions={1}, use_global_device_ids=true | all-gather | bytes 327680 | tf_op jit(solution)/shard_map/all_gather | solution.py:128
  37.6 1.1 %fusion.24 = bf16[1,8,32,2,4,64]{5,2,4,1,3,0:T(8,128)(2,1)} fusion(f32[1,8,32,2,4,64]{5,4,3,2,1,0:T(4,128)S(1)} %reshape.337, f32[64]{0:T(128)S(1)} %copy-done.5, f32[8,32,2,4]{1,3,0,2:T(4,128)S(1)} %copy.45), kind=kLoop, calls=%fused_computation.45 | loop fusion | flops 393216 | bytes 794880 | tf_op jit(solution)/shard_map/convert_element_type | solution.py:45
  38.7 0.0 all-to-all-done
  38.7 1.0 %copy.52 = bf16[4,1,2,8,8,256]{5,4,0,3,2,1:T(8,128)(2,1)S(1)} copy(bf16[4,1,2,8,8,256]{5,4,3,2,1,0:T(8,128)(2,1)} %bitcast.32) | data formatting | bytes 524288 | tf_op jit(solution)/shard_map/reshape | solution.py:125
  39.7 15.5 %while.20 = (s32[]{:T(128)}, f32[1,2,4,8,32]{4,2,3,1,0:T(4,128)S(1)}, f32[1,2,4,8,32]{4,2,3,1,0:T(4,128)S(1)}, f32[1,2,4,8,32,64]{5,4,3,2,1,0:T(8,128)S(1)}, s32...) while((s32[]{:T(128)}, ...), condition=%wide.region_7.8_spmd.clone, body=%wide.region_3.7_spmd.clone.sunk | while | flops 140261664 | bytes 9158459 | solution.py:120
  39.7 0.1 mul.341
  39.8 0.1 compare_reduce_fusion.2
  39.9 0.1 sub.166
  40.0 0.1 fusion.48
  40.1 0.1 subtract_convert_fusion.2
  40.2 1.7 %fusion.49 = (f32[2,4,8,32]{3,1,2,0:T(4,128)S(1)}, f32[1,2,4,8,32,256]{5,4,2,3,1,0:T(8,128)S(1)}) fusion(f32[8,32,256]{2,1,0:T(8,128)S(1)} %subtract_convert_fusion.2, f32[2,4]{1,0:T(2,128)S(1)} %mul.341, bf16[1,8,32,2,4,64]{5,2,4,1,3,0:T(8,128)(2,1)} %get-tuple-element.433, bf16[1,1024,2,64]{1,3,2,0:T(8,128)(2,1)S(1)} %get-tuple-element.432, ...), kind=kOutput, calls=%fused_computation.58.clone.1 | convolution fusion | flops 70252544 | bytes 2761732 | tf_op jit(solution)/shard_map/while/body/eval_jaxpr/sbqkgd,snkd->skgbqn/dot_general | solution.py:72
  42.0 0.8 %fusion.51 = (bf16[2,4,8,32,256]{4,3,1,2,0:T(8,128)(2,1)S(1)}, f32[2,4,8,32]{3,1,2,0:T(4,128)S(1)}) fusion(f32[1,2,4,8,32,256]{5,4,2,3,1,0:T(8,128)S(1)} %get-tuple-element.395, f32[2,4,8,32]{3,1,2,0:T(4,128)S(1)} %bitcast.97, pred[8,32,256]{2,1,0:T(8,128)(4,1)S(1)} %fusion.48), kind=kLoop, calls=%fused_computation.9.clone.1 | loop fusion | flops 2095104 | bytes 3227648 | tf_op jit(solution)/shard_map/reshape.269
  42.8 0.1 bitcast_add_fusion.2
  42.9 0.7 fusion.52
  43.6 0.1 mul.341
  43.7 0.1 compare_reduce_fusion.2
  43.8 0.1 sub.166
  43.9 0.1 fusion.48
  44.0 0.1 subtract_convert_fusion.2
  44.1 1.7 %fusion.49 = (f32[2,4,8,32]{3,1,2,0:T(4,128)S(1)}, f32[1,2,4,8,32,256]{5,4,2,3,1,0:T(8,128)S(1)}) fusion(f32[8,32,256]{2,1,0:T(8,128)S(1)} %subtract_convert_fusion.2, f32[2,4]{1,0:T(2,128)S(1)} %mul.341, bf16[1,8,32,2,4,64]{5,2,4,1,3,0:T(8,128)(2,1)} %get-tuple-element.433, bf16[1,1024,2,64]{1,3,2,0:T(8,128)(2,1)S(1)} %get-tuple-element.432, ...), kind=kOutput, calls=%fused_computation.58.clone.1 | convolution fusion | flops 70252544 | bytes 2761732 | tf_op jit(solution)/shard_map/while/body/eval_jaxpr/sbqkgd,snkd->skgbqn/dot_general | solution.py:72
  45.9 0.8 %fusion.51 = (bf16[2,4,8,32,256]{4,3,1,2,0:T(8,128)(2,1)S(1)}, f32[2,4,8,32]{3,1,2,0:T(4,128)S(1)}) fusion(f32[1,2,4,8,32,256]{5,4,2,3,1,0:T(8,128)S(1)} %get-tuple-element.395, f32[2,4,8,32]{3,1,2,0:T(4,128)S(1)} %bitcast.97, pred[8,32,256]{2,1,0:T(8,128)(4,1)S(1)} %fusion.48), kind=kLoop, calls=%fused_computation.9.clone.1 | loop fusion | flops 2095104 | bytes 3227648 | tf_op jit(solution)/shard_map/reshape.269
  46.7 0.1 bitcast_add_fusion.2
  46.8 0.7 fusion.52
  47.5 0.1 mul.341
  47.6 0.1 compare_reduce_fusion.2
  47.7 0.1 sub.166
  47.8 0.1 fusion.48
  47.9 0.1 subtract_convert_fusion.2
  48.0 1.7 %fusion.49 = (f32[2,4,8,32]{3,1,2,0:T(4,128)S(1)}, f32[1,2,4,8,32,256]{5,4,2,3,1,0:T(8,128)S(1)}) fusion(f32[8,32,256]{2,1,0:T(8,128)S(1)} %subtract_convert_fusion.2, f32[2,4]{1,0:T(2,128)S(1)} %mul.341, bf16[1,8,32,2,4,64]{5,2,4,1,3,0:T(8,128)(2,1)} %get-tuple-element.433, bf16[1,1024,2,64]{1,3,2,0:T(8,128)(2,1)S(1)} %get-tuple-element.432, ...), kind=kOutput, calls=%fused_computation.58.clone.1 | convolution fusion | flops 70252544 | bytes 2761732 | tf_op jit(solution)/shard_map/while/body/eval_jaxpr/sbqkgd,snkd->skgbqn/dot_general | solution.py:72
  49.8 0.8 %fusion.51 = (bf16[2,4,8,32,256]{4,3,1,2,0:T(8,128)(2,1)S(1)}, f32[2,4,8,32]{3,1,2,0:T(4,128)S(1)}) fusion(f32[1,2,4,8,32,256]{5,4,2,3,1,0:T(8,128)S(1)} %get-tuple-element.395, f32[2,4,8,32]{3,1,2,0:T(4,128)S(1)} %bitcast.97, pred[8,32,256]{2,1,0:T(8,128)(4,1)S(1)} %fusion.48), kind=kLoop, calls=%fused_computation.9.clone.1 | loop fusion | flops 2095104 | bytes 3227648 | tf_op jit(solution)/shard_map/reshape.269
  50.7 0.1 bitcast_add_fusion.2
  50.7 0.6 fusion.52
  51.4 0.1 mul.341
  51.5 0.1 compare_reduce_fusion.2
  51.6 0.1 sub.166
  51.7 0.1 fusion.48
  51.8 0.1 subtract_convert_fusion.2
  51.9 1.7 %fusion.49 = (f32[2,4,8,32]{3,1,2,0:T(4,128)S(1)}, f32[1,2,4,8,32,256]{5,4,2,3,1,0:T(8,128)S(1)}) fusion(f32[8,32,256]{2,1,0:T(8,128)S(1)} %subtract_convert_fusion.2, f32[2,4]{1,0:T(2,128)S(1)} %mul.341, bf16[1,8,32,2,4,64]{5,2,4,1,3,0:T(8,128)(2,1)} %get-tuple-element.433, bf16[1,1024,2,64]{1,3,2,0:T(8,128)(2,1)S(1)} %get-tuple-element.432, ...), kind=kOutput, calls=%fused_computation.58.clone.1 | convolution fusion | flops 70252544 | bytes 2761732 | tf_op jit(solution)/shard_map/while/body/eval_jaxpr/sbqkgd,snkd->skgbqn/dot_general | solution.py:72
  53.7 0.8 %fusion.51 = (bf16[2,4,8,32,256]{4,3,1,2,0:T(8,128)(2,1)S(1)}, f32[2,4,8,32]{3,1,2,0:T(4,128)S(1)}) fusion(f32[1,2,4,8,32,256]{5,4,2,3,1,0:T(8,128)S(1)} %get-tuple-element.395, f32[2,4,8,32]{3,1,2,0:T(4,128)S(1)} %bitcast.97, pred[8,32,256]{2,1,0:T(8,128)(4,1)S(1)} %fusion.48), kind=kLoop, calls=%fused_computation.9.clone.1 | loop fusion | flops 2095104 | bytes 3227648 | tf_op jit(solution)/shard_map/reshape.269
  54.5 0.1 bitcast_add_fusion.2
  54.6 0.6 fusion.52
  55.2 0.0 copy-start.1
  55.3 0.3 fusion.26
  55.6 0.4 copy.48
  56.0 0.3 convert_element_type.91
  56.4 0.1 copy-done.1
  56.5 1.3 %fusion.19 = bf16[1024,256]{0,1:T(8,128)(2,1)} fusion(bf16[256,512]{1,0:T(8,128)(2,1)S(1)} %convert_element_type.91, bf16[512,1024]{1,0:T(8,128)(2,1)S(1)} %copy-done.1), kind=kOutput, calls=%fused_computation.38 | convolution fusion | flops 268697600 | bytes 1835008 | tf_op jit(solution)/shard_map/dot_general | solution.py:139
  57.7 0.0 reduce-scatter.2.cloned.1.call-update
  57.8 0.7 reshape.339
  58.4 8.7 %reduce-scatter.2.cloned.1.call-done = bf16[512,256]{0,1:T(8,128)(2,1)} async-done(((bf16[1024,256]{0,1:T(8,128)(2,1)}), bf16[512,256]{0,1:T(8,128)(2,1)}) %reduce-scatter.2.cloned.1.call-update) | async-done | bytes 262160 | tf_op jit(solution)/shard_map/reduce_scatter | solution.py:141
  (45 shorter events, 0.4 us)
Async XLA Ops:
  7.2 12.3 %copy-start = (bf16[1024,512]{1,0:T(8,128)(2,1)S(1)}, bf16[1024,512]{1,0:T(8,128)(2,1)}, u32[]{:S(2)}) copy-start(bf16[1024,512]{1,0:T(8,128)(2,1)} %param.13) | copy-start | bytes 3145732
  7.2 11.3 %copy-start.3 = (f32[1024]{0:T(1024)S(1)}, f32[1024]{0:T(1024)}, u32[]{:S(2)}) copy-start(f32[1024]{0:T(1024)} %param.12) | copy-start | bytes 12292
  7.2 4.2 %copy-start.4 = (f32[64]{0:T(128)S(1)}, f32[64]{0:T(128)}, u32[]{:S(2)}) copy-start(f32[64]{0:T(128)} %param.17) | copy-start | bytes 772
  7.2 11.3 %copy-start.6 = (bf16[1024,128]{1,0:T(8,128)(2,1)S(1)}, bf16[1024,128]{1,0:T(8,128)(2,1)}, u32[]{:S(2)}) copy-start(bf16[1024,128]{1,0:T(8,128)(2,1)} %param.15) | copy-start | bytes 786436
  12.3 26.4 %all-to-all-start = ((bf16[4,1,256,2,64]{2,4,3,1,0:T(8,128)(2,1)}), bf16[4,1,256,2,64]{2,4,3,1,0:T(8,128)(2,1)}, u32[]{:S(2)}, u32[]{:S(2)}) async-start(bf16[4,1,256,2,64]{2,4,3,1,0:T(8,128)(2,1)} %stack.2), calls=%async_computation | async-start | bytes 524288 | tf_op jit(solution)/shard_map/all_to_all | solution.py:126
  18.5 48.7 %reduce-scatter.2.cloned.1.call-start = ((), (), s32[]{:S(2)}) async-start(), calls=%async_computation.2 | async-start | bytes 786432 | tf_op jit(solution)/shard_map/reduce_scatter | solution.py:141
  20.8 16.8 %copy-start.5 = (f32[64]{0:T(128)S(1)}, f32[64]{0:T(128)}, u32[]{:S(2)}) copy-start(f32[64]{0:T(128)} %param.16) | copy-start | bytes 772
  21.0 18.6 %copy-start.2 = (s32[1,8,16]{2,1,0:T(8,128)S(1)}, s32[1,8,16]{2,1,0:T(8,128)}, u32[]{:S(2)}) copy-start(s32[1,8,16]{2,1,0:T(8,128)} %param.19) | copy-start | bytes 1540
  55.2 1.2 %copy-start.1 = (bf16[512,1024]{1,0:T(8,128)(2,1)S(1)}, bf16[512,1024]{1,0:T(8,128)(2,1)}, u32[]{:S(2)}) copy-start(bf16[512,1024]{1,0:T(8,128)(2,1)} %param.18) | copy-start | bytes 3145732
Sparse Core Ops, SparseCore 0:
  57.9 9.2 reduce-scatter.1
